TPU v7x, 32 devices: a whole 2x2x4 slice. The times are simulated.
32 devices in a mesh: rep: 2 (over y), fs: 4 (over z), tp: 4 (over x, core).
Axes of the slice: x: 2, y: 2, z: 4, core: 2. Of those that a mesh axis runs over, the one named last changes fastest.
Arguments:
- activations: bfloat16 [8, 256, 2048], P(('rep', 'fs'), None, 'tp'), may hold values from -15 to 15
- norm_gain: float32 [2048], replicated, may hold values from 0.1 to 1.9
- w_value: bfloat16 [2048, 2048], P('fs', 'tp'), may hold values from -0.125 to 0.125
- w_gate_conv: bfloat16 [2048, 2048], P('fs', 'tp'), may hold values from -0.125 to 0.125
- conv_weight: float32 [31, 2048], P(None, 'tp'), may hold values from -3 to 3
- chan_gain: float32 [2048], P('tp'), may hold values from 0.1 to 1.9
- w_conv_out: bfloat16 [2048, 2048], P('tp', 'fs'), may hold values from -0.125 to 0.125
- mix_gain: float32 [2048], replicated, may hold values from 0.1 to 1.9
- w_gate: bfloat16 [2048, 3072], P('fs', 'tp'), may hold values from -0.125 to 0.125
- w_up: bfloat16 [2048, 3072], P('fs', 'tp'), may hold values from -0.125 to 0.125
- w_down: bfloat16 [3072, 2048], P('tp', 'fs'), may hold values from -0.109375 to 0.109375
- final_gain: float32 [2048], P('tp'), may hold values from 0.1 to 1.9
Outputs:
- result: bfloat16 [8, 256, 2048], P(('rep', 'fs'), None, 'tp')
All inputs are finite; a program needn't handle non-finite values.
Results may differ from a plain program's by a relative error of at most 0.013.
Values may be sent and summed in bfloat16 or wider, within the bound.
A program may use at most 64 MiB of HBM per device.

v0:
```python
import jax
import jax.numpy as jnp
from jax import lax
from jax.sharding import PartitionSpec as P

EPS = 1e-06


def body(
    activations,
    norm_gain,
    w_value,
    w_gate_conv,
    conv_weight,
    chan_gain,
    w_conv_out,
    mix_gain,
    w_gate,
    w_up,
    w_down,
    final_gain,
):
    batch, length, local_width = activations.shape
    width = local_width * lax.axis_size("tp")
    count = batch * length
    residual = activations.reshape(count, local_width).astype(jnp.float32)
    raw_in = lax.all_gather(
        activations.reshape(count, local_width), "tp", axis=1, tiled=True
    ).astype(jnp.float32)
    in_mean = jnp.mean(raw_in * raw_in, axis=1, keepdims=True)
    rows_in = (raw_in * lax.rsqrt(in_mean + EPS) * norm_gain).astype(jnp.bfloat16)
    chan_local = w_value.shape[1]
    pieces = (
        lax.all_gather(w_value, "fs", axis=0, tiled=True),
        lax.all_gather(w_gate_conv, "fs", axis=0, tiled=True),
    )
    columns = rows_in
    value = jnp.dot(columns, pieces[0], preferred_element_type=jnp.float32)
    gate_conv = jnp.dot(columns, pieces[1], preferred_element_type=jnp.float32)
    glu = (value * jax.nn.sigmoid(gate_conv)).reshape(batch, length, chan_local)
    taps = conv_weight.shape[0]
    padded = jnp.pad(glu, ((0, 0), (taps - 1, 0), (0, 0)))
    conv = lax.conv_general_dilated(
        padded,
        conv_weight[:, None, :],
        (1,),
        "VALID",
        dimension_numbers=("NWC", "WIO", "NWC"),
        feature_group_count=chan_local,
        precision=lax.Precision.HIGHEST,
    ).reshape(count, chan_local)
    chan_total = chan_local * lax.axis_size("tp")
    mean = lax.psum(jnp.sum(conv, axis=1), "tp") / chan_total
    centered = conv - mean[:, None]
    spread = lax.psum(jnp.sum(centered * centered, axis=1), "tp") / chan_total
    act = jax.nn.silu(centered * lax.rsqrt(spread + EPS)[:, None] * chan_gain).astype(jnp.bfloat16)
    conv_terms = jnp.dot(
        act,
        lax.all_gather(w_conv_out, "fs", axis=1, tiled=True),
        preferred_element_type=jnp.float32,
    )
    conv_out = lax.psum_scatter(
        conv_terms.astype(jnp.bfloat16), "tp", scatter_dimension=1, tiled=True
    ).astype(jnp.float32)
    first = (residual + conv_out).astype(jnp.bfloat16)
    first_f = first.astype(jnp.float32)
    raw_mid = lax.all_gather(first, "tp", axis=1, tiled=True).astype(jnp.float32)
    mid_mean = jnp.mean(raw_mid * raw_mid, axis=1, keepdims=True)
    rows_mid = (raw_mid * lax.rsqrt(mid_mean + EPS) * mix_gain).astype(jnp.bfloat16)
    hidden_local = w_gate.shape[1]
    zero_hidden = jnp.zeros((count, hidden_local), jnp.float32)
    pieces = (
        lax.all_gather(w_gate, "fs", axis=0, tiled=True),
        lax.all_gather(w_up, "fs", axis=0, tiled=True),
    )
    columns = lax.slice_in_dim(rows_mid, 0, pieces[0].shape[0], axis=1)
    gate = zero_hidden + jnp.dot(columns, pieces[0], preferred_element_type=jnp.float32)
    up = zero_hidden + jnp.dot(columns, pieces[1], preferred_element_type=jnp.float32)
    hidden = (jax.nn.silu(gate) * up).astype(jnp.bfloat16)
    ff_terms = jnp.dot(
        hidden, lax.all_gather(w_down, "fs", axis=1, tiled=True), preferred_element_type=jnp.float32
    )
    ff_out = lax.psum_scatter(
        ff_terms.astype(jnp.bfloat16), "tp", scatter_dimension=1, tiled=True
    ).astype(jnp.float32)
    second = first_f + ff_out
    out_total = lax.psum(jnp.sum(second * second, axis=1), "tp")
    result = (second * lax.rsqrt(out_total / width + EPS)[:, None] * final_gain).astype(
        jnp.bfloat16
    )
    return result.reshape(batch, length, local_width)


def solution(mesh):
    in_specs = (
        P(("rep", "fs"), None, "tp"),
        P(),
        P("fs", "tp"),
        P("fs", "tp"),
        P(None, "tp"),
        P("tp"),
        P("tp", "fs"),
        P(),
        P("fs", "tp"),
        P("fs", "tp"),
        P("tp", "fs"),
        P("tp"),
    )
    out_specs = P(("rep", "fs"), None, "tp")
    return jax.shard_map(body, mesh=mesh, in_specs=in_specs, out_specs=out_specs, check_vma=False)
```

profile of v0, /device:TPU:0, one launch (start us, length us, event | category | flops | bytes accessed | tf_op | source)
XLA Modules:
  0.0 451.0 jit_solution(17801474472369738869)
XLA Ops:
  6.5 0.0 copy-start
  6.5 0.0 all-gather.24.cloned.1.call-start
  6.5 0.7 all-gather.24.cloned.1.call-update
  7.3 0.0 all-gather.12.cloned.1.call-start
  7.3 0.7 all-gather.12.cloned.1.call-update
  8.0 0.0 all-gather.10.cloned.1.call-start
  8.1 0.7 all-gather.10.cloned.1.call-update
  8.7 0.0 all-gather.14.cloned.1.call-start
  8.8 0.5 all-gather.14.cloned.1.call-update
  9.3 0.0 reduce-scatter.3.cloned.1.call-start
  9.4 19.0 %all-gather.24.cloned.1.call-done = bf16[1,256,2048]{2,1,0:T(8,128)(2,1)} async-done(((bf16[1,256,512]{2,1,0:T(8,128)(2,1)}), bf16[1,256,2048]{2,1,0:T(8,128)(2,1)}) %all-gather.24.cloned.1.call-update) | async-done | bytes 1048592 | tf_op jit(solution)/shard_map/all_gather | solution.py:27
  28.4 1.5 fusion.3
  29.9 0.0 copy-start.4
  29.9 45.7 %all-gather.12.cloned.1.call-done = bf16[2048,512]{1,0:T(8,128)(2,1)} async-done(((bf16[512,512]{1,0:T(8,128)(2,1)}), bf16[2048,512]{1,0:T(8,128)(2,1)}) %all-gather.12.cloned.1.call-update) | async-done | bytes 2097168 | tf_op jit(solution)/shard_map/all_gather | solution.py:35
  75.6 0.0 copy-done.6
  75.6 2.8 fusion.10
  78.4 43.3 %all-gather.10.cloned.1.call-done = bf16[2048,512]{1,0:T(8,128)(2,1)} async-done(((bf16[512,512]{1,0:T(8,128)(2,1)}), bf16[2048,512]{1,0:T(8,128)(2,1)}) %all-gather.10.cloned.1.call-update) | async-done | bytes 2097168 | tf_op jit(solution)/shard_map/all_gather | solution.py:34
  121.7 0.0 copy-done.4
  121.7 2.3 fusion.7
  124.0 0.0 copy-start.9
  124.0 0.1 pad.2
  124.1 0.7 reshape.42
  124.8 0.2 copy.18
  125.0 0.1 slice.2
  125.1 0.0 copy-done
  125.1 0.0 copy-done.9
  125.1 1.2 convolution_select_fusion
  126.3 0.3 copy.20
  126.7 0.1 reshape.46
  126.8 0.1 slice_reduce_fusion
  126.9 6.4 %psum.21 = f32[256]{0:T(256)S(1)} all-reduce(f32[256]{0:T(256)S(1)} %slice_reduce_fusion), channel_id=1, replica_groups=mesh['rep'=2,'fs'=4,'tp'=4] {'tp'}, use_global_device_ids=true, to_apply=%region_2.3 | all-reduce | flops 256 | bytes 2048 | tf_op jit(solution)/shard_map/psum | solution.py:53
  133.3 0.2 multiply_reduce_fusion.1
  133.5 6.3 %psum.22 = f32[256]{0:T(256)S(1)} all-reduce(f32[256]{0:T(256)S(1)} %multiply_reduce_fusion.1), channel_id=1, replica_groups=mesh['rep'=2,'fs'=4,'tp'=4] {'tp'}, use_global_device_ids=true, to_apply=%region_4.5 | all-reduce | flops 256 | bytes 2048 | tf_op jit(solution)/shard_map/psum | solution.py:55
  139.8 27.8 %all-gather.14.cloned.1.call-done = bf16[512,2048]{1,0:T(8,128)(2,1)} async-done(((bf16[512,512]{1,0:T(8,128)(2,1)}), bf16[512,2048]{1,0:T(8,128)(2,1)}) %all-gather.14.cloned.1.call-update) | async-done | bytes 2097168 | tf_op jit(solution)/shard_map/all_gather | solution.py:59
  167.6 3.4 convolution_convert_fusion
  171.0 0.0 reduce-scatter.3.cloned.1.call-update
  171.1 0.0 copy-start.7
  171.1 0.0 all-gather.16.cloned.1.call-start
  171.1 23.7 %reduce-scatter.3.cloned.1.call-done = bf16[256,512]{1,0:T(8,128)(2,1)} async-done(((bf16[256,2048]{1,0:T(8,128)(2,1)}), bf16[256,512]{1,0:T(8,128)(2,1)}) %reduce-scatter.3.cloned.1.call-update) | async-done | bytes 262160 | tf_op jit(solution)/shard_map/reduce_scatter | solution.py:62
  194.8 1.7 fusion.17
  196.5 0.0 all-gather.16.cloned.1.call-update
  196.6 0.0 all-gather.18.cloned.1.call-start
  196.6 0.7 all-gather.18.cloned.1.call-update
  197.3 0.0 all-gather.20.cloned.1.call-start
  197.4 0.7 all-gather.20.cloned.1.call-update
  198.1 0.0 all-gather.22.cloned.1.call-start
  198.1 0.7 all-gather.22.cloned.1.call-update
  198.8 0.0 reduce-scatter.5.cloned.1.call-start
  198.8 14.6 %all-gather.16.cloned.1.call-done = bf16[256,2048]{1,0:T(8,128)(2,1)} async-done(((bf16[256,512]{1,0:T(8,128)(2,1)}), bf16[256,2048]{1,0:T(8,128)(2,1)}) %all-gather.16.cloned.1.call-update) | async-done | bytes 1048592 | tf_op jit(solution)/shard_map/all_gather | solution.py:67
  213.4 1.5 fusion
  215.0 63.5 %all-gather.18.cloned.1.call-done = bf16[2048,768]{1,0:T(8,128)(2,1)} async-done(((bf16[512,768]{1,0:T(8,128)(2,1)}), bf16[2048,768]{1,0:T(8,128)(2,1)}) %all-gather.18.cloned.1.call-update) | async-done | bytes 3145744 | tf_op jit(solution)/shard_map/all_gather | solution.py:73
  278.5 3.2 fusion.23
  281.7 0.0 copy-start.1
  281.7 0.0 copy-start.5
  281.8 60.4 %all-gather.20.cloned.1.call-done = bf16[2048,768]{1,0:T(8,128)(2,1)} async-done(((bf16[512,768]{1,0:T(8,128)(2,1)}), bf16[2048,768]{1,0:T(8,128)(2,1)}) %all-gather.20.cloned.1.call-update) | async-done | bytes 3145744 | tf_op jit(solution)/shard_map/all_gather | solution.py:74
  342.2 63.7 %all-gather.22.cloned.1.call-done = bf16[768,2048]{1,0:T(8,128)(2,1)} async-done(((bf16[768,512]{1,0:T(8,128)(2,1)}), bf16[768,2048]{1,0:T(8,128)(2,1)}) %all-gather.22.cloned.1.call-update) | async-done | bytes 3145744 | tf_op jit(solution)/shard_map/all_gather | solution.py:81
  405.9 0.0 copy-done.3
  405.9 6.0 %convolution_convert_fusion.1 = bf16[256,2048]{1,0:T(8,128)(2,1)} fusion(bf16[768,2048]{1,0:T(8,128)(2,1)} %all-gather.22.cloned.1.call-done, bf16[2048,768]{1,0:T(8,128)(2,1)} %all-gather.20.cloned.1.call-done, f32[256,768]{1,0:T(8,128)S(1)} %fusion.23, bf16[256,2048]{1,0:T(8,128)(2,1)S(1)} %copy-done.3, f32[2048]{0:T(1024)S(1)} %copy-done.7, ...), kind=kOutput, calls=%fused_computation.5 | convolution fusion | flops 1614413824 | bytes 9184256 | tf_op jit(solution)/shard_map/dot_general | solution.py:80
  411.9 0.0 reduce-scatter.5.cloned.1.call-update
  411.9 23.6 %reduce-scatter.5.cloned.1.call-done = bf16[256,512]{1,0:T(8,128)(2,1)} async-done(((bf16[256,2048]{1,0:T(8,128)(2,1)}), bf16[256,512]{1,0:T(8,128)(2,1)}) %reduce-scatter.5.cloned.1.call-update) | async-done | bytes 262160 | tf_op jit(solution)/shard_map/reduce_scatter | solution.py:83
  435.5 1.1 multiply_reduce_fusion
  436.6 5.8 %psum.23 = f32[256]{0:T(256)S(1)} all-reduce(f32[256]{0:T(256)S(1)} %multiply_reduce_fusion), channel_id=1, replica_groups=mesh['rep'=2,'fs'=4,'tp'=4] {'tp'}, use_global_device_ids=true, to_apply=%region_9.10 | all-reduce | flops 256 | bytes 2048 | tf_op jit(solution)/shard_map/psum | solution.py:87
  442.4 0.0 copy-done.5
  442.4 1.8 fusion.25
  (13 shorter events, 0.1 us)
Async XLA Ops:
  6.5 118.5 %copy-start = (f32[31,512]{1,0:T(8,128)S(1)}, f32[31,512]{1,0:T(8,128)}, u32[]{:S(2)}) copy-start(f32[31,512]{1,0:T(8,128)} %param.16) | copy-start | bytes 190468
  6.5 69.1 %copy-start.6 = (f32[2048]{0:T(1024)S(1)}, f32[2048]{0:T(1024)}, u32[]{:S(2)}) copy-start(f32[2048]{0:T(1024)} %param.13) | copy-start | bytes 24580
  6.5 21.8 %all-gather.24.cloned.1.call-start = ((), (), s32[]{:S(2)}) async-start(), calls=%async_computation.11 | async-start | bytes 1310720 | tf_op jit(solution)/shard_map/all_gather | solution.py:27
  7.3 68.3 %all-gather.12.cloned.1.call-start = ((), (), s32[]{:S(2)}) async-start(), calls=%async_computation.3 | async-start | bytes 2621440 | tf_op jit(solution)/shard_map/all_gather | solution.py:35
  8.0 113.7 %all-gather.10.cloned.1.call-start = ((), (), s32[]{:S(2)}) async-start(), calls=%async_computation.2 | async-start | bytes 2621440 | tf_op jit(solution)/shard_map/all_gather | solution.py:34
  8.7 158.9 %all-gather.14.cloned.1.call-start = ((), (), s32[]{:S(2)}) async-start(), calls=%async_computation.4 | async-start | bytes 2621440 | tf_op jit(solution)/shard_map/all_gather | solution.py:59
  9.3 185.5 %reduce-scatter.3.cloned.1.call-start = ((), (), s32[]{:S(2)}) async-start(), calls=%async_computation.5 | async-start | bytes 1310720 | tf_op jit(solution)/shard_map/reduce_scatter | solution.py:62
  29.9 91.8 %copy-start.4 = (bf16[1,256,2048]{2,1,0:T(8,128)(2,1)S(1)}, bf16[1,256,2048]{2,1,0:T(8,128)(2,1)}, u32[]{:S(2)}) copy-start(bf16[1,256,2048]{2,1,0:T(8,128)(2,1)} %all-gather.24.cloned.1.call-done) | copy-start | bytes 3145732
  124.0 1.0 copy-start.9
  126.3 41.3 %copy-start.8 = (f32[512]{0:T(512)S(1)}, f32[512]{0:T(512)}, u32[]{:S(2)}) copy-start(f32[512]{0:T(512)} %param.17) | copy-start | bytes 6148
  139.8 55.1 %copy-start.2 = (bf16[1,256,512]{2,1,0:T(8,128)(2,1)S(1)}, bf16[1,256,512]{2,1,0:T(8,128)(2,1)}, u32[]{:S(2)}) copy-start(bf16[1,256,512]{2,1,0:T(8,128)(2,1)} %param.12) | copy-start | bytes 786436
  171.1 107.4 %copy-start.7 = (f32[2048]{0:T(1024)S(1)}, f32[2048]{0:T(1024)}, u32[]{:S(2)}) copy-start(f32[2048]{0:T(1024)} %param.19) | copy-start | bytes 24580
  171.1 42.4 %all-gather.16.cloned.1.call-start = ((), (), s32[]{:S(2)}) async-start(), calls=%async_computation.6 | async-start | bytes 1310720 | tf_op jit(solution)/shard_map/all_gather | solution.py:67
  196.6 81.9 %all-gather.18.cloned.1.call-start = ((), (), s32[]{:S(2)}) async-start(), calls=%async_computation.7 | async-start | bytes 3932160 | tf_op jit(solution)/shard_map/all_gather | solution.py:73
  197.3 144.8 %all-gather.20.cloned.1.call-start = ((), (), s32[]{:S(2)}) async-start(), calls=%async_computation.8 | async-start | bytes 3932160 | tf_op jit(solution)/shard_map/all_gather | solution.py:74
  198.1 207.8 %all-gather.22.cloned.1.call-start = ((), (), s32[]{:S(2)}) async-start(), calls=%async_computation.9 | async-start | bytes 3932160 | tf_op jit(solution)/shard_map/all_gather | solution.py:81
  198.8 236.7 %reduce-scatter.5.cloned.1.call-start = ((), (), s32[]{:S(2)}) async-start(), calls=%async_computation.10 | async-start | bytes 1310720 | tf_op jit(solution)/shard_map/reduce_scatter | solution.py:83
  214.9 190.9 %copy-start.3 = (bf16[256,2048]{1,0:T(8,128)(2,1)S(1)}, bf16[256,2048]{1,0:T(8,128)(2,1)}, u32[]{:S(2)}) copy-start(bf16[256,2048]{1,0:T(8,128)(2,1)} %all-gather.16.cloned.1.call-done) | copy-start | bytes 3145732
  281.7 153.8 %copy-start.1 = (bf16[256,512]{1,0:T(8,128)(2,1)S(1)}, bf16[256,512]{1,0:T(8,128)(2,1)}, u32[]{:S(2)}) copy-start(bf16[256,512]{1,0:T(8,128)(2,1)} %fusion.17) | copy-start | bytes 786436
  281.7 160.6 %copy-start.5 = (f32[512]{0:T(512)S(1)}, f32[512]{0:T(512)}, u32[]{:S(2)}) copy-start(f32[512]{0:T(512)} %param.23) | copy-start | bytes 6148
Sparse Core Ops, SparseCore 0:
  8.9 19.4 all-gather.23
  29.9 45.6 all-gather.11
  77.2 44.4 all-gather.9
  123.1 44.4 all-gather.13
  171.2 23.6 reduce-scatter.2
  196.7 16.6 all-gather.15
  215.0 63.4 all-gather.17
  280.0 62.0 all-gather.19
  343.7 62.0 all-gather.21
  412.0 23.4 reduce-scatter.4
where the time goes:
time: 451 us
  waiting for transfers between devices  390 us (86%)
  matrix products  19 us (4%)
  blocking collectives  18.4 us (4%)
  between operations  13.7 us (3%)
  other arithmetic  7.97 us (2%)
    all_gather x1, waiting for transfers between devices, body(): lax.all_gather(w_down, 'fs', axis=1, tiled=True)  63.7 us
    all_gather x1, waiting for transfers between devices, body(): lax.all_gather(w_gate, 'fs', axis=0, tiled=True)  63.5 us
    all_gather x1, waiting for transfers between devices, body(): lax.all_gather(w_up, 'fs', axis=0, tiled=True)  60.4 us
    all_gather x1, waiting for transfers between devices, body(): lax.all_gather(w_gate_conv, 'fs', axis=0, tiled=True)  45.7 us
    all_gather x1, waiting for transfers between devices, body(): lax.all_gather(w_value, 'fs', axis=0, tiled=True)  43.3 us
    all_gather x1, waiting for transfers between devices, body(): lax.all_gather(w_conv_out, 'fs', axis=1, tiled=True)  27.8 us
    reduce_scatter x1, waiting for transfers between devices, body(): lax.psum_scatter(conv_terms.astype(jnp.bfloat16), 'tp', scatter_dimension...  23.7 us
    reduce_scatter x1, waiting for transfers between devices, body(): lax.psum_scatter(ff_terms.astype(jnp.bfloat16), 'tp', scatter_dimension=1...  23.6 us
  transfers between devices with their start and end apart: 10, of which 10 were waited for; matrix products, arithmetic and copies ran while one was open for 3% of the time, Pallas kernels for 0%

commit v1 on v0

--- a/solution.py
+++ b/solution.py
@@ -56,7 +56,7 @@
     act = jax.nn.silu(centered * lax.rsqrt(spread + EPS)[:, None] * chan_gain).astype(jnp.bfloat16)
     conv_terms = jnp.dot(
         act,
-        lax.all_gather(w_conv_out, "fs", axis=1, tiled=True),
+        jnp.concatenate(lax.all_gather(w_conv_out, "fs"), axis=1),
         preferred_element_type=jnp.float32,
     )
     conv_out = lax.psum_scatter(

time: 451 us -> 453 us (level)
  no operation moved by 1% of the time
where the time goes in v1:
time: 453 us; the launch traced here: 452 us
  waiting for transfers between devices  390 us (86%)
  blocking collectives  18.4 us (4%)
  matrix products  17.4 us (4%)
  between operations  13.7 us (3%)
  other arithmetic  7.97 us (2%)
    all_gather x1, waiting for transfers between devices, body(): lax.all_gather(w_down, 'fs', axis=1, tiled=True)  63.7 us
    all_gather x1, waiting for transfers between devices, body(): lax.all_gather(w_gate, 'fs', axis=0, tiled=True)  63.5 us
    all_gather x1, waiting for transfers between devices, body(): lax.all_gather(w_up, 'fs', axis=0, tiled=True)  60.4 us
    all_gather x1, waiting for transfers between devices, body(): lax.all_gather(w_gate_conv, 'fs', axis=0, tiled=True)  45.7 us
    all_gather x1, waiting for transfers between devices, body(): lax.all_gather(w_value, 'fs', axis=0, tiled=True)  43.3 us
    all_gather x1, waiting for transfers between devices, body(): lax.all_gather(w_conv_out, 'fs')  27.9 us
    reduce_scatter x1, waiting for transfers between devices, body(): lax.psum_scatter(conv_terms.astype(jnp.bfloat16), 'tp', scatter_dimension...  23.7 us
    reduce_scatter x1, waiting for transfers between devices, body(): lax.psum_scatter(ff_terms.astype(jnp.bfloat16), 'tp', scatter_dimension=1...  23.6 us
  transfers between devices with their start and end apart: 10, of which 10 were waited for; matrix products, arithmetic and copies ran while one was open for 3% of the time, Pallas kernels for 0%

profile of v1, /device:TPU:0, one launch (start us, length us, event | category | flops | bytes accessed | tf_op | source)
XLA Modules:
  0.0 452.2 jit_solution(11743184909991592886)
XLA Ops:
  6.5 0.0 copy-start
  6.5 0.0 all-gather.23.cloned.1.call-start
  6.5 0.7 all-gather.23.cloned.1.call-update
  7.3 0.0 all-gather.13.cloned.1.call-start
  7.3 0.7 all-gather.13.cloned.1.call-update
  8.0 0.0 all-gather.11.cloned.1.call-start
  8.1 0.7 all-gather.11.cloned.1.call-update
  8.7 0.0 all-gather.25.cloned.1.call-start
  8.8 0.5 all-gather.25.cloned.1.call-update
  9.3 0.0 reduce-scatter.3.cloned.1.call-start
  9.4 19.0 %all-gather.23.cloned.1.call-done = bf16[1,256,2048]{2,1,0:T(8,128)(2,1)} async-done(((bf16[1,256,512]{2,1,0:T(8,128)(2,1)}), bf16[1,256,2048]{2,1,0:T(8,128)(2,1)}) %all-gather.23.cloned.1.call-update) | async-done | bytes 1048592 | tf_op jit(solution)/shard_map/all_gather | solution.py:27
  28.4 1.5 fusion.3
  29.9 0.0 copy-start.4
  29.9 45.7 %all-gather.13.cloned.1.call-done = bf16[2048,512]{1,0:T(8,128)(2,1)} async-done(((bf16[512,512]{1,0:T(8,128)(2,1)}), bf16[2048,512]{1,0:T(8,128)(2,1)}) %all-gather.13.cloned.1.call-update) | async-done | bytes 2097168 | tf_op jit(solution)/shard_map/all_gather | solution.py:35
  75.6 0.0 copy-done.6
  75.6 2.8 fusion.10
  78.4 43.3 %all-gather.11.cloned.1.call-done = bf16[2048,512]{1,0:T(8,128)(2,1)} async-done(((bf16[512,512]{1,0:T(8,128)(2,1)}), bf16[2048,512]{1,0:T(8,128)(2,1)}) %all-gather.11.cloned.1.call-update) | async-done | bytes 2097168 | tf_op jit(solution)/shard_map/all_gather | solution.py:34
  121.7 0.0 copy-done.4
  121.7 2.3 fusion.7
  124.0 0.0 copy-start.9
  124.0 0.1 pad.2
  124.1 0.7 reshape.67
  124.8 0.2 copy.21
  125.0 0.1 slice.2
  125.1 0.0 copy-done
  125.1 1.2 convolution_select_fusion
  126.3 0.3 copy.23
  126.7 0.1 reshape.71
  126.7 0.1 slice_reduce_fusion
  126.9 6.4 %psum.21 = f32[256]{0:T(256)S(1)} all-reduce(f32[256]{0:T(256)S(1)} %slice_reduce_fusion), channel_id=1, replica_groups=mesh['rep'=2,'fs'=4,'tp'=4] {'tp'}, use_global_device_ids=true, to_apply=%region_2.3 | all-reduce | flops 256 | bytes 2048 | tf_op jit(solution)/shard_map/psum | solution.py:53
  133.3 0.2 fusion.19
  133.5 6.3 %psum.22 = f32[256]{0:T(256)S(1)} all-reduce(f32[256]{0:T(256)S(1)} %fusion.19), channel_id=1, replica_groups=mesh['rep'=2,'fs'=4,'tp'=4] {'tp'}, use_global_device_ids=true, to_apply=%region_4.5 | all-reduce | flops 256 | bytes 2048 | tf_op jit(solution)/shard_map/psum | solution.py:55
  139.7 27.9 %all-gather.25.cloned.1.call-done = bf16[2048,512]{1,0:T(8,128)(2,1)} async-done(((bf16[512,512]{1,0:T(8,128)(2,1)}), bf16[2048,512]{1,0:T(8,128)(2,1)}) %all-gather.25.cloned.1.call-update) | async-done | bytes 2097168 | tf_op jit(solution)/shard_map/all_gather | solution.py:59
  167.6 2.8 copy.24
  170.4 0.0 copy-start.2
  170.4 1.8 convolution_convert_fusion
  172.2 0.0 reduce-scatter.3.cloned.1.call-update
  172.3 0.0 copy-start.7
  172.3 0.0 all-gather.15.cloned.1.call-start
  172.3 23.7 %reduce-scatter.3.cloned.1.call-done = bf16[256,512]{1,0:T(8,128)(2,1)} async-done(((bf16[256,2048]{1,0:T(8,128)(2,1)}), bf16[256,512]{1,0:T(8,128)(2,1)}) %reduce-scatter.3.cloned.1.call-update) | async-done | bytes 262160 | tf_op jit(solution)/shard_map/reduce_scatter | solution.py:62
  196.0 1.7 fusion.17
  197.7 0.0 all-gather.15.cloned.1.call-update
  197.8 0.0 all-gather.17.cloned.1.call-start
  197.8 0.7 all-gather.17.cloned.1.call-update
  198.5 0.0 all-gather.19.cloned.1.call-start
  198.6 0.7 all-gather.19.cloned.1.call-update
  199.3 0.0 all-gather.21.cloned.1.call-start
  199.3 0.7 all-gather.21.cloned.1.call-update
  200.0 0.0 reduce-scatter.5.cloned.1.call-start
  200.0 14.6 %all-gather.15.cloned.1.call-done = bf16[256,2048]{1,0:T(8,128)(2,1)} async-done(((bf16[256,512]{1,0:T(8,128)(2,1)}), bf16[256,2048]{1,0:T(8,128)(2,1)}) %all-gather.15.cloned.1.call-update) | async-done | bytes 1048592 | tf_op jit(solution)/shard_map/all_gather | solution.py:67
  214.6 1.5 fusion
  216.1 63.5 %all-gather.17.cloned.1.call-done = bf16[2048,768]{1,0:T(8,128)(2,1)} async-done(((bf16[512,768]{1,0:T(8,128)(2,1)}), bf16[2048,768]{1,0:T(8,128)(2,1)}) %all-gather.17.cloned.1.call-update) | async-done | bytes 3145744 | tf_op jit(solution)/shard_map/all_gather | solution.py:73
  279.7 3.2 fusion.25
  282.9 0.0 copy-start.1
  282.9 0.0 copy-start.5
  282.9 60.4 %all-gather.19.cloned.1.call-done = bf16[2048,768]{1,0:T(8,128)(2,1)} async-done(((bf16[512,768]{1,0:T(8,128)(2,1)}), bf16[2048,768]{1,0:T(8,128)(2,1)}) %all-gather.19.cloned.1.call-update) | async-done | bytes 3145744 | tf_op jit(solution)/shard_map/all_gather | solution.py:74
  343.3 63.7 %all-gather.21.cloned.1.call-done = bf16[768,2048]{1,0:T(8,128)(2,1)} async-done(((bf16[768,512]{1,0:T(8,128)(2,1)}), bf16[768,2048]{1,0:T(8,128)(2,1)}) %all-gather.21.cloned.1.call-update) | async-done | bytes 3145744 | tf_op jit(solution)/shard_map/all_gather | solution.py:81
  407.0 0.0 copy-done.3
  407.0 6.0 %convolution_convert_fusion.1 = bf16[256,2048]{1,0:T(8,128)(2,1)} fusion(bf16[768,2048]{1,0:T(8,128)(2,1)} %all-gather.21.cloned.1.call-done, bf16[2048,768]{1,0:T(8,128)(2,1)} %all-gather.19.cloned.1.call-done, f32[256,768]{1,0:T(8,128)S(1)} %fusion.25, bf16[256,2048]{1,0:T(8,128)(2,1)S(1)} %copy-done.3, f32[2048]{0:T(1024)S(1)} %copy-done.7, ...), kind=kOutput, calls=%fused_computation.5 | convolution fusion | flops 1614413824 | bytes 9184256 | tf_op jit(solution)/shard_map/dot_general | solution.py:80
  413.1 0.0 reduce-scatter.5.cloned.1.call-update
  413.1 23.6 %reduce-scatter.5.cloned.1.call-done = bf16[256,512]{1,0:T(8,128)(2,1)} async-done(((bf16[256,2048]{1,0:T(8,128)(2,1)}), bf16[256,512]{1,0:T(8,128)(2,1)}) %reduce-scatter.5.cloned.1.call-update) | async-done | bytes 262160 | tf_op jit(solution)/shard_map/reduce_scatter | solution.py:83
  436.7 1.1 multiply_reduce_fusion
  437.8 5.8 %psum.23 = f32[256]{0:T(256)S(1)} all-reduce(f32[256]{0:T(256)S(1)} %multiply_reduce_fusion), channel_id=1, replica_groups=mesh['rep'=2,'fs'=4,'tp'=4] {'tp'}, use_global_device_ids=true, to_apply=%region_9.10 | all-reduce | flops 256 | bytes 2048 | tf_op jit(solution)/shard_map/psum | solution.py:87
  443.6 1.8 fusion.27
  (14 shorter events, 0.1 us)
Async XLA Ops:
  6.5 118.5 %copy-start = (f32[31,512]{1,0:T(8,128)S(1)}, f32[31,512]{1,0:T(8,128)}, u32[]{:S(2)}) copy-start(f32[31,512]{1,0:T(8,128)} %param.16) | copy-start | bytes 190468
  6.5 69.1 %copy-start.6 = (f32[2048]{0:T(1024)S(1)}, f32[2048]{0:T(1024)}, u32[]{:S(2)}) copy-start(f32[2048]{0:T(1024)} %param.13) | copy-start | bytes 24580
  6.5 21.8 %all-gather.23.cloned.1.call-start = ((), (), s32[]{:S(2)}) async-start(), calls=%async_computation.10 | async-start | bytes 1310720 | tf_op jit(solution)/shard_map/all_gather | solution.py:27
  7.3 68.3 %all-gather.13.cloned.1.call-start = ((), (), s32[]{:S(2)}) async-start(), calls=%async_computation.3 | async-start | bytes 2621440 | tf_op jit(solution)/shard_map/all_gather | solution.py:35
  8.0 113.7 %all-gather.11.cloned.1.call-start = ((), (), s32[]{:S(2)}) async-start(), calls=%async_computation.2 | async-start | bytes 2621440 | tf_op jit(solution)/shard_map/all_gather | solution.py:34
  8.7 158.9 %all-gather.25.cloned.1.call-start = ((), (), s32[]{:S(2)}) async-start(), calls=%async_computation.11 | async-start | bytes 2621440 | tf_op jit(solution)/shard_map/all_gather | solution.py:59
  9.3 186.7 %reduce-scatter.3.cloned.1.call-start = ((), (), s32[]{:S(2)}) async-start(), calls=%async_computation.4 | async-start | bytes 1310720 | tf_op jit(solution)/shard_map/reduce_scatter | solution.py:62
  29.9 91.8 %copy-start.4 = (bf16[1,256,2048]{2,1,0:T(8,128)(2,1)S(1)}, bf16[1,256,2048]{2,1,0:T(8,128)(2,1)}, u32[]{:S(2)}) copy-start(bf16[1,256,2048]{2,1,0:T(8,128)(2,1)} %all-gather.23.cloned.1.call-done) | copy-start | bytes 3145732
  124.0 1.0 copy-start.9
  167.6 2.8 copy-start.8
  170.4 25.6 %copy-start.2 = (bf16[1,256,512]{2,1,0:T(8,128)(2,1)S(1)}, bf16[1,256,512]{2,1,0:T(8,128)(2,1)}, u32[]{:S(2)}) copy-start(bf16[1,256,512]{2,1,0:T(8,128)(2,1)} %param.12) | copy-start | bytes 786436
  172.3 107.4 %copy-start.7 = (f32[2048]{0:T(1024)S(1)}, f32[2048]{0:T(1024)}, u32[]{:S(2)}) copy-start(f32[2048]{0:T(1024)} %param.19) | copy-start | bytes 24580
  172.3 42.3 %all-gather.15.cloned.1.call-start = ((), (), s32[]{:S(2)}) async-start(), calls=%async_computation.5 | async-start | bytes 1310720 | tf_op jit(solution)/shard_map/all_gather | solution.py:67
  197.8 81.9 %all-gather.17.cloned.1.call-start = ((), (), s32[]{:S(2)}) async-start(), calls=%async_computation.6 | async-start | bytes 3932160 | tf_op jit(solution)/shard_map/all_gather | solution.py:73
  198.5 144.8 %all-gather.19.cloned.1.call-start = ((), (), s32[]{:S(2)}) async-start(), calls=%async_computation.7 | async-start | bytes 3932160 | tf_op jit(solution)/shard_map/all_gather | solution.py:74
  199.3 207.8 %all-gather.21.cloned.1.call-start = ((), (), s32[]{:S(2)}) async-start(), calls=%async_computation.8 | async-start | bytes 3932160 | tf_op jit(solution)/shard_map/all_gather | solution.py:81
  200.0 236.7 %reduce-scatter.5.cloned.1.call-start = ((), (), s32[]{:S(2)}) async-start(), calls=%async_computation.9 | async-start | bytes 1310720 | tf_op jit(solution)/shard_map/reduce_scatter | solution.py:83
  216.1 190.9 %copy-start.3 = (bf16[256,2048]{1,0:T(8,128)(2,1)S(1)}, bf16[256,2048]{1,0:T(8,128)(2,1)}, u32[]{:S(2)}) copy-start(bf16[256,2048]{1,0:T(8,128)(2,1)} %all-gather.15.cloned.1.call-done) | copy-start | bytes 3145732
  282.9 153.8 %copy-start.1 = (bf16[256,512]{1,0:T(8,128)(2,1)S(1)}, bf16[256,512]{1,0:T(8,128)(2,1)}, u32[]{:S(2)}) copy-start(bf16[256,512]{1,0:T(8,128)(2,1)} %fusion.17) | copy-start | bytes 786436
  282.9 160.6 %copy-start.5 = (f32[512]{0:T(512)S(1)}, f32[512]{0:T(512)}, u32[]{:S(2)}) copy-start(f32[512]{0:T(512)} %param.23) | copy-start | bytes 6148
Sparse Core Ops, SparseCore 0:
  8.9 19.4 all-gather.22
  29.9 45.6 all-gather.12
  77.2 44.4 all-gather.10
  123.1 44.4 all-gather.24
  172.4 23.5 reduce-scatter.2
  197.9 16.6 all-gather.14
  216.2 63.4 all-gather.16
  281.2 62.0 all-gather.18
  344.9 62.0 all-gather.20
  413.2 23.4 reduce-scatter.4
